TPU v7x, 32 devices: a whole 2x2x4 slice. The times are simulated.
32 devices in a mesh: sp: 4 (over z), fs: 4 (over y, x), tp: 2 (over core).
Axes of the slice: x: 2, y: 2, z: 4, core: 2. Of those that a mesh axis runs over, the one named last changes fastest.
Arguments:
- tokens: bfloat16 [4096, 2048], P(('fs', 'sp')), parts along dimension 0, may hold values from -6 to 6
- norm_gain: float32 [2048], replicated, may hold values from 0.1 to 1.9
- w_query: bfloat16 [2048, 1024], P('sp', 'tp'), may hold values from -0.080939698 to 0.080939698
- w_key: bfloat16 [2048, 256], P('sp', 'tp'), may hold values from -0.080939698 to 0.080939698
- w_value: bfloat16 [2048, 256], P('sp', 'tp'), may hold values from -0.125 to 0.125
- w_conv_in: bfloat16 [2048, 1024], P('sp', 'tp'), may hold values from -0.125 to 0.125
- w_conv_gate: bfloat16 [2048, 1024], P('sp', 'tp'), may hold values from -0.125 to 0.125
- sink_logit: float32 [16], P('tp'), may hold values from 2 to 6
- conv_taps: float32 [31, 1024], P(None, 'tp'), may hold values from -5.3881591 to 5.3881591
- conv_bias: float32 [1024], P('tp'), may hold values from -0.9 to 5.9
- channel_gain: float32 [1024], P('tp'), may hold values from 0.1 to 1.9
- channel_shift: float32 [1024], P('tp'), may hold values from -3 to 3
- w_attn_out: bfloat16 [1024, 2048], P(None, 'sp'), may hold values from -1.5 to 1.5
- w_conv_out: bfloat16 [1024, 2048], P(None, 'sp'), may hold values from -0.1875 to 0.1875
Outputs:
- output: bfloat16 [4096, 2048], P(('fs', 'sp', 'tp')), parts along dimension 0
There are 4 independent parts, one for each index of `fs`. A program takes and returns all parts, laid end to end along the dimension named above; an argument that names none is the same for every part. Nothing has to cross between parts.
All inputs are finite; a program needn't handle non-finite values.
Results may differ from a plain program's by a relative error of at most 0.011.
Values may be sent and summed in bfloat16 or wider, within the bound.
A program may use at most 64 MiB of HBM per device.

v0:
```python
import jax
import jax.numpy as jnp
from jax import lax
from jax.sharding import PartitionSpec as P

HEAD_DIM = 64
WINDOW = 128
GRID_W = 64
EPSILON = 1e-06
NEGATIVE = -1e30
ROPE_BASE = 10000.0


def padded(block, sides, width):
    for axis, dim in sides:
        count = lax.axis_size(axis)
        forward = [(i, i + 1) for i in range(count - 1)]
        backward = [(target, source) for source, target in forward]
        low = lax.ppermute(
            lax.slice_in_dim(block, block.shape[dim] - width, None, axis=dim), axis, forward
        )
        high = lax.ppermute(lax.slice_in_dim(block, 0, width, axis=dim), axis, backward)
        block = jnp.concatenate([low, block, high], axis=dim)
    return block


def rotate_pairs(values, positions):
    middle = values.shape[-1] // 2
    inverse = ROPE_BASE ** (-jnp.arange(middle, dtype=jnp.float32) / middle)
    angles = positions.astype(jnp.float32)[:, None] * inverse[None, :]
    cosine = jnp.cos(angles)[:, None, :]
    sine_table = jnp.sin(angles)[:, None, :]
    leading = values[..., :middle]
    trailing = values[..., middle:]
    return jnp.concatenate(
        [leading * cosine - trailing * sine_table, leading * sine_table + trailing * cosine],
        axis=-1,
    )


def grid_rotate(values, positions):
    middle = values.shape[-1] // 2
    return jnp.concatenate(
        [
            rotate_pairs(values[..., :middle], positions // GRID_W),
            rotate_pairs(values[..., middle:], positions % GRID_W),
        ],
        axis=-1,
    )


def local(
    tokens,
    norm_gain,
    w_query,
    w_key,
    w_value,
    w_conv_in,
    w_conv_gate,
    sink_logit,
    conv_taps,
    conv_bias,
    channel_gain,
    channel_shift,
    w_attn_out,
    w_conv_out,
):
    rows_here = tokens.shape[0]
    offset = lax.axis_index("sp") * rows_here
    total = rows_here * lax.axis_size("sp")
    tp_count = lax.axis_size("tp")
    token_float = tokens.astype(jnp.float32)
    normed = (
        token_float
        * lax.rsqrt(jnp.mean(token_float * token_float, axis=-1, keepdims=True) + EPSILON)
        * norm_gain[None, :]
    ).astype(jnp.bfloat16)
    head_cols = w_query.shape[1]
    kv_cols = w_key.shape[1]
    chan_cols = w_conv_in.shape[1]
    piece_query = lax.all_gather(w_query, "sp", axis=0, tiled=True)
    piece_key = lax.all_gather(w_key, "sp", axis=0, tiled=True)
    piece_value = lax.all_gather(w_value, "sp", axis=0, tiled=True)
    piece_conv = lax.all_gather(w_conv_in, "sp", axis=0, tiled=True)
    piece_gate = lax.all_gather(w_conv_gate, "sp", axis=0, tiled=True)
    query_acc = jnp.dot(normed, piece_query, preferred_element_type=jnp.float32)
    pair_acc = jnp.dot(
        normed,
        jnp.concatenate([piece_key, piece_value], axis=1),
        preferred_element_type=jnp.float32,
    )
    conv_acc = jnp.dot(
        normed,
        jnp.concatenate([piece_conv, piece_gate], axis=1),
        preferred_element_type=jnp.float32,
    )
    positions = offset + jnp.arange(rows_here, dtype=jnp.int32)
    heads_here = head_cols // HEAD_DIM
    kv_here = kv_cols // HEAD_DIM
    group = heads_here // kv_here
    query = grid_rotate(query_acc.reshape(rows_here, heads_here, HEAD_DIM), positions).astype(
        jnp.bfloat16
    )
    keys = grid_rotate(pair_acc[:, :kv_cols].reshape(rows_here, kv_here, HEAD_DIM), positions)
    keys = keys.astype(jnp.bfloat16).reshape(rows_here, kv_cols)
    values = pair_acc[:, kv_cols:].astype(jnp.bfloat16)
    stacked = jnp.concatenate([keys, values], axis=1)
    extended = padded(stacked, (("sp", 0),), WINDOW)
    block = min(rows_here, 512)
    span = block + 2 * WINDOW
    sinks = sink_logit.reshape(kv_here, group)[:, :, None, None]
    queries = query.reshape(block, kv_here, group, HEAD_DIM)
    near_keys = extended[:, :kv_cols].reshape(span, kv_here, HEAD_DIM)
    near_values = extended[:, kv_cols:].reshape(span, kv_here, HEAD_DIM)
    scores = jnp.einsum(
        "qkgd,skd->kgqs", queries, near_keys, preferred_element_type=jnp.float32
    ) * HEAD_DIM ** (-0.5)
    query_pos = offset + 0 + jnp.arange(block, dtype=jnp.int32)
    key_pos = offset + 0 - WINDOW + jnp.arange(span, dtype=jnp.int32)
    valid = (
        (jnp.abs(query_pos[:, None] - key_pos[None, :]) <= WINDOW)
        & (key_pos[None, :] >= 0)
        & (key_pos[None, :] < total)
    )
    scores = jnp.where(valid[None, None], scores, NEGATIVE)
    top = jnp.maximum(jnp.max(scores, axis=-1, keepdims=True), sinks)
    raised = jnp.exp(scores - top)
    denominator = jnp.sum(raised, axis=-1, keepdims=True) + jnp.exp(sinks - top)
    probs = (raised / denominator).astype(jnp.bfloat16)
    mixed = jnp.einsum("kgqs,skd->qkgd", probs, near_values, preferred_element_type=jnp.float32)
    outputs = mixed.astype(jnp.bfloat16).reshape(block, head_cols)
    glu = (conv_acc[:, :chan_cols] * jax.nn.sigmoid(conv_acc[:, chan_cols:])).astype(jnp.bfloat16)
    reach = conv_taps.shape[0] // 2
    rims = padded(glu, (("sp", 0),), reach)
    filtered = jnp.zeros((rows_here, chan_cols), jnp.float32) + conv_bias[None, :]
    for shift_index in range(conv_taps.shape[0]):
        filtered = filtered + conv_taps[shift_index][None, :] * rims[
            shift_index : shift_index + rows_here
        ].astype(jnp.float32)
    channel_total = chan_cols * tp_count
    centre = lax.psum(jnp.sum(filtered, axis=-1), "tp")[:, None] / channel_total
    centred = filtered - centre
    spread = lax.psum(jnp.sum(centred * centred, axis=-1), "tp")[:, None] / channel_total
    conv_out = jax.nn.silu(
        centred * lax.rsqrt(spread + EPSILON) * channel_gain[None, :] + channel_shift[None, :]
    ).astype(jnp.bfloat16)
    features = jnp.concatenate([outputs, conv_out], axis=1)
    tp_here = lax.axis_index("tp")
    own_rows = jnp.concatenate(
        [
            lax.dynamic_slice_in_dim(w_attn_out, tp_here * head_cols, head_cols, 0),
            lax.dynamic_slice_in_dim(w_conv_out, tp_here * chan_cols, chan_cols, 0),
        ],
        axis=0,
    )
    own_whole = lax.all_gather(own_rows, "sp", axis=1, tiled=True)
    result = lax.psum_scatter(
        jnp.dot(features, own_whole, preferred_element_type=jnp.float32).astype(jnp.bfloat16),
        "tp",
        scatter_dimension=0,
        tiled=True,
    )
    return result


def solution(mesh):
    in_specs = (
        P(("fs", "sp"), None),
        P(),
        P("sp", "tp"),
        P("sp", "tp"),
        P("sp", "tp"),
        P("sp", "tp"),
        P("sp", "tp"),
        P("tp"),
        P(None, "tp"),
        P("tp"),
        P("tp"),
        P("tp"),
        P(None, "sp"),
        P(None, "sp"),
    )
    out_specs = P(("fs", "sp", "tp"), None)
    return jax.shard_map(local, mesh=mesh, in_specs=in_specs, out_specs=out_specs, check_vma=False)
```

profile of v0, /device:TPU:0, one launch (start us, length us, event | category | flops | bytes accessed | tf_op | source)
XLA Modules:
  0.0 263.5 jit_solution(13735289390232705822)
XLA Ops:
  8.8 1.3 constant_dynamic-slice_fusion
  10.1 1.0 pad_maximum_fusion
  11.6 23.1 %all_gather.18 = bf16[2048,128]{1,0:T(8,128)(2,1)S(1)} all-gather(bf16[512,128]{1,0:T(8,128)(2,1)S(1)} %copy-done.1), channel_id=1, replica_groups=mesh['sp'=4,'fs'=4,'tp'=2] {'sp'}, dimensions={0}, use_global_device_ids=true | all-gather | bytes 655360 | tf_op jit(solution)/shard_map/all_gather | solution.py:82
  34.7 21.7 %all_gather.19 = bf16[2048,128]{1,0:T(8,128)(2,1)S(1)} all-gather(bf16[512,128]{1,0:T(8,128)(2,1)S(1)} %copy-done.2), channel_id=1, replica_groups=mesh['sp'=4,'fs'=4,'tp'=2] {'sp'}, dimensions={0}, use_global_device_ids=true | all-gather | bytes 655360 | tf_op jit(solution)/shard_map/all_gather | solution.py:83
  57.4 1.5 collective-permute-start
  58.9 1.3 collective-permute-start.1
  60.7 1.5 collective-permute-done
  62.2 7.0 %collective-permute-done.1 = bf16[128,256]{0,1:T(8,128)(2,1)S(1)} collective-permute-done((bf16[128,256]{0,1:T(8,128)(2,1)S(1)}, bf16[128,256]{0,1:T(8,128)(2,1)S(1)}, u32[]{:S(2)}, u32[]{:S(2)}) %collective-permute-start.1) | collective-permute-done | bytes 65568 | tf_op jit(solution)/shard_map/ppermute | solution.py:22
  69.2 1.9 all-gather.7.cloned.1.call-done
  71.1 47.3 %all-gather.9.cloned.1.call-done = bf16[2048,512]{1,0:T(8,128)(2,1)} async-done(((bf16[512,512]{1,0:T(8,128)(2,1)}), bf16[2048,512]{1,0:T(8,128)(2,1)}) %all-gather.9.cloned.1.call-update) | async-done | bytes 2097168 | tf_op jit(solution)/shard_map/all_gather | solution.py:85
  118.4 3.5 %fusion = f32[256,1024]{1,0:T(8,128)S(1)} fusion(bf16[2048,512]{1,0:T(8,128)(2,1)} %all-gather.9.cloned.1.call-done, bf16[2048,512]{1,0:T(8,128)(2,1)} %all-gather.7.cloned.1.call-done, bf16[256,2048]{1,0:T(8,128)(2,1)S(1)} %copy-done, f32[2048]{0:T(1024)S(1)} %copy-done.7, f32[256]{0:T(256)S(1)} %add_rsqrt_fusion.1), kind=kOutput, calls=%fused_computation | convolution fusion | flops 1084227584 | bytes 6300672 | tf_op jit(solution)/shard_map/dot_general | solution.py:92
  122.1 2.1 collective-permute-start.2
  124.2 1.3 collective-permute-start.3
  125.5 39.2 %all-gather.5.cloned.1.call-done = bf16[2048,512]{1,0:T(8,128)(2,1)} async-done(((bf16[512,512]{1,0:T(8,128)(2,1)}), bf16[2048,512]{1,0:T(8,128)(2,1)}) %all-gather.5.cloned.1.call-update) | async-done | bytes 2097168 | tf_op jit(solution)/shard_map/all_gather | solution.py:81
  164.6 2.6 fusion.74
  167.3 0.8 fusion.5
  168.2 0.9 fusion.4
  169.3 1.2 fusion.10
  170.7 3.1 %fusion.77 = (f32[256]{0:T(256)S(1)}, f32[256,512]{1,0:T(8,128)S(1)}) fusion(bf16[15,512]{1,0:T(8,128)(2,1)S(1)} %collective-permute-done.3, bf16[256,512]{1,0:T(8,128)(2,1)S(1)} %fusion.22, f32[512]{0:T(512)S(1)} %bitcast.106, f32[512]{0:T(512)S(1)} %bitcast.107, f32[512]{0:T(512)S(1)} %bitcast.78, f32[512]{0:T(512)S(1)} %bitcast.79, f32[512]{0:T(512)S(1)} %bitcast.80, ...), kind=kLoop, calls=%fused_computation.167 | loop fusion | flops 24116992 | bytes 883712 | tf_op jit(solution)/shard_map/reduce_sum | solution.py:141
  173.8 2.5 psum.14
  176.4 2.5 psum.15
  179.2 66.3 %all-gather.11.cloned.1.call-done = bf16[1024,2048]{1,0:T(8,128)(2,1)} async-done(((bf16[1024,512]{1,0:T(8,128)(2,1)}), bf16[1024,2048]{1,0:T(8,128)(2,1)}) %all-gather.11.cloned.1.call-update) | async-done | bytes 4194320 | tf_op jit(solution)/shard_map/all_gather | solution.py:156
  245.5 4.5 %convolution_convert_fusion = bf16[256,2048]{1,0:T(8,128)(2,1)} fusion(bf16[1024,2048]{1,0:T(8,128)(2,1)} %all-gather.11.cloned.1.call-done, bf16[256,512]{1,0:T(8,128)(2,1)S(1)} %multiply_convert_fusion, bf16[256,512]{1,0:T(8,128)(2,1)S(1)} %copy.27), kind=kOutput, calls=%fused_computation.11 | convolution fusion | flops 1075314688 | bytes 5767168 | tf_op jit(solution)/shard_map/dot_general | solution.py:158
  249.9 7.0 %reduce-scatter.2.cloned.1.call-done = bf16[128,2048]{1,0:T(8,128)(2,1)} async-done(((bf16[256,2048]{1,0:T(8,128)(2,1)}), bf16[128,2048]{1,0:T(8,128)(2,1)}) %reduce-scatter.2.cloned.1.call-update) | async-done | bytes 524304 | tf_op jit(solution)/shard_map/reduce_scatter | solution.py:157
  (60 shorter events, 5.1 us)
Async XLA Ops:
  6.5 4.7 %copy-start = (bf16[256,2048]{1,0:T(8,128)(2,1)S(1)}, bf16[256,2048]{1,0:T(8,128)(2,1)}, u32[]{:S(2)}) copy-start(bf16[256,2048]{1,0:T(8,128)(2,1)} %param.14) | copy-start | bytes 3145732
  6.5 5.0 %copy-start.1 = (bf16[512,128]{1,0:T(8,128)(2,1)S(1)}, bf16[512,128]{1,0:T(8,128)(2,1)}, u32[]{:S(2)}) copy-start(bf16[512,128]{1,0:T(8,128)(2,1)} %param.17) | copy-start | bytes 393220
  6.5 28.1 %copy-start.2 = (bf16[512,128]{1,0:T(8,128)(2,1)S(1)}, bf16[512,128]{1,0:T(8,128)(2,1)}, u32[]{:S(2)}) copy-start(bf16[512,128]{1,0:T(8,128)(2,1)} %param.18) | copy-start | bytes 393220
  6.5 64.6 %all-gather.7.cloned.1.call-start = ((), (), s32[]{:S(2)}) async-start(), calls=%async_computation.2 | async-start | bytes 2621440 | tf_op jit(solution)/shard_map/all_gather | solution.py:84
  7.3 111.1 %all-gather.9.cloned.1.call-start = ((), (), s32[]{:S(2)}) async-start(), calls=%async_computation.3 | async-start | bytes 2621440 | tf_op jit(solution)/shard_map/all_gather | solution.py:85
  8.0 48.4 %copy-start.7 = (f32[2048]{0:T(1024)S(1)}, f32[2048]{0:T(1024)}, u32[]{:S(2)}) copy-start(f32[2048]{0:T(1024)} %param.15) | copy-start | bytes 24580
  8.0 156.6 %all-gather.5.cloned.1.call-start = ((), (), s32[]{:S(2)}) async-start(), calls=%async_computation.1 | async-start | bytes 2621440 | tf_op jit(solution)/shard_map/all_gather | solution.py:81
  8.8 236.7 %all-gather.11.cloned.1.call-start = ((), (), s32[]{:S(2)}) async-start(), calls=%async_computation.4 | async-start | bytes 5242880 | tf_op jit(solution)/shard_map/all_gather | solution.py:156
  11.1 49.1 %copy-start.3 = (f32[31,512]{1,0:T(8,128)S(1)}, f32[31,512]{1,0:T(8,128)}, u32[]{:S(2)}) copy-start(f32[31,512]{1,0:T(8,128)} %param.22) | copy-start | bytes 190468
  11.1 49.5 %copy-start.8 = (f32[8]{0:T(128)S(1)}, f32[8]{0:T(128)}, u32[]{:S(2)}) copy-start(f32[8]{0:T(128)} %param.21) | copy-start | bytes 100
  11.2 245.8 %reduce-scatter.2.cloned.1.call-start = ((), (), s32[]{:S(2)}) async-start(), calls=%async_computation.5 | async-start | bytes 1572864 | tf_op jit(solution)/shard_map/reduce_scatter | solution.py:157
  57.4 4.8 %collective-permute-start = (bf16[128,256]{0,1:T(8,128)(2,1)S(1)}, bf16[128,256]{0,1:T(8,128)(2,1)S(1)}, u32[]{:S(2)}, u32[]{:S(2)}) collective-permute-start(bf16[128,256]{0,1:T(8,128)(2,1)S(1)} %get-tuple-element.21), channel_id=1, source_target_pairs={{0,8},{8,16},{16,24},{1,9},{9,17},{17,25},{2,10},{10,18},{18,26},{... | collective-permute-start | bytes 196616 | tf_op jit(solution)/shard_map/ppermute | solution.py:19
  58.9 10.3 %collective-permute-start.1 = (bf16[128,256]{0,1:T(8,128)(2,1)S(1)}, bf16[128,256]{0,1:T(8,128)(2,1)S(1)}, u32[]{:S(2)}, u32[]{:S(2)}) collective-permute-start(bf16[128,256]{0,1:T(8,128)(2,1)S(1)} %get-tuple-element.22), channel_id=1, source_target_pairs={{8,0},{16,8},{24,16},{9,1},{17,9},{25,17},{10,2},{18,10},{26,18},{... | collective-permute-start | bytes 196616 | tf_op jit(solution)/shard_map/ppermute | solution.py:22
  122.1 48.6 %collective-permute-start.2 = (bf16[15,512]{1,0:T(8,128)(2,1)S(1)}, bf16[15,512]{1,0:T(8,128)(2,1)S(1)}, u32[]{:S(2)}, u32[]{:S(2)}) collective-permute-start(bf16[15,512]{1,0:T(8,128)(2,1)S(1)} %get-tuple-element.15), channel_id=1, source_target_pairs={{0,8},{8,16},{16,24},{1,9},{9,17},{17,25},{2,10},{10,18},{18,26},{... | collective-permute-start | bytes 46088 | tf_op jit(solution)/shard_map/ppermute | solution.py:19
  124.2 46.5 %collective-permute-start.3 = (bf16[15,512]{1,0:T(8,128)(2,1)S(1)}, bf16[15,512]{1,0:T(8,128)(2,1)S(1)}, u32[]{:S(2)}, u32[]{:S(2)}) collective-permute-start(bf16[15,512]{1,0:T(8,128)(2,1)S(1)} %get-tuple-element.16), channel_id=1, source_target_pairs={{8,0},{16,8},{24,16},{9,1},{17,9},{25,17},{10,2},{18,10},{26,18},{... | collective-permute-start | bytes 46088 | tf_op jit(solution)/shard_map/ppermute | solution.py:22
  169.2 1.4 copy-start.4
  169.2 9.7 %copy-start.5 = (f32[512]{0:T(512)S(1)}, f32[512]{0:T(512)}, u32[]{:S(2)}) copy-start(f32[512]{0:T(512)} %param.25) | copy-start | bytes 6148
  169.2 9.7 %copy-start.6 = (f32[512]{0:T(512)S(1)}, f32[512]{0:T(512)}, u32[]{:S(2)}) copy-start(f32[512]{0:T(512)} %param.24) | copy-start | bytes 6148
Sparse Core Ops, SparseCore 0:
  8.9 62.1 all-gather.6
  72.7 45.6 all-gather.8
  120.0 44.6 all-gather.4
  166.1 79.3 all-gather.10
  250.1 6.8 reduce-scatter.1
where the time goes:
time: 264 us
  waiting for transfers between devices  172 us (65%)
  blocking collectives  49.7 us (19%)
  between operations  13.5 us (5%)
  matrix products  13.3 us (5%)
  other arithmetic  6.78 us (3%)
  starting transfers between devices  6.35 us (2%)
    all_gather x1, waiting for transfers between devices, local(): own_whole = lax.all_gather(own_rows, 'sp', axis=1, tiled=True)  66.3 us
    all_gather x1, waiting for transfers between devices, local(): piece_gate = lax.all_gather(w_conv_gate, 'sp', axis=0, tiled=True)  47.3 us
    all_gather x1, waiting for transfers between devices, local(): piece_query = lax.all_gather(w_query, 'sp', axis=0, tiled=True)  39.2 us
    all_gather x1, blocking collectives, local(): piece_key = lax.all_gather(w_key, 'sp', axis=0, tiled=True)  23.1 us
    all_gather x1, blocking collectives, local(): piece_value = lax.all_gather(w_value, 'sp', axis=0, tiled=True)  21.7 us
    reduce_scatter x1, waiting for transfers between devices, local(): lax.psum_scatter(jnp.dot(features, own_whole, preferred_element_type=jnp....  7.04 us
    ppermute x2, waiting for transfers between devices, padded(): lax.ppermute(lax.slice_in_dim(block, 0, width, axis=dim), axis, backward)  6.99 us
  transfers between devices with their start and end apart: 9, of which 7 were waited for; matrix products, arithmetic and copies ran while one was open for 7% of the time, Pallas kernels for 0%

commit v1 on v0

--- a/solution.py
+++ b/solution.py
@@ -79,7 +79,13 @@
     kv_cols = w_key.shape[1]
     chan_cols = w_conv_in.shape[1]
     piece_query = lax.all_gather(w_query, "sp", axis=0, tiled=True)
-    piece_key = lax.all_gather(w_key, "sp", axis=0, tiled=True)
+    devices = lax.axis_size("sp")
+    moving, pieces = (w_key, [w_key])
+    for _ in range(devices - 1):
+        moving = lax.ppermute(moving, "sp", [(i_2, (i_2 + 1) % devices) for i_2 in range(devices)])
+        pieces.insert(0, moving)
+    line = jnp.concatenate(pieces, axis=0)
+    piece_key = jnp.roll(line, (lax.axis_index("sp") + 1) * w_key.shape[0], axis=0)
     piece_value = lax.all_gather(w_value, "sp", axis=0, tiled=True)
     piece_conv = lax.all_gather(w_conv_in, "sp", axis=0, tiled=True)
     piece_gate = lax.all_gather(w_conv_gate, "sp", axis=0, tiled=True)

time: 264 us -> 262 us (level)
  blocking collectives: 49.7 us -> 31 us
  waiting for transfers between devices: 172 us -> 185 us
  starting transfers between devices: 6.35 us -> 10.3 us
    all_gather x1 -> x0, blocking collectives: 23.1 us -> none  [local(): piece_key = lax.all_gather(w_key, 'sp', axis=0, tiled=True)]
    ppermute x0 -> x3, waiting for transfers between devices: none -> 10.2 us  [local(): lax.ppermute(moving, 'sp', [(i_2, (i_2 + 1) % devices) for i_2 in range(d...]
    all_gather x1, blocking collectives: 21.7 us -> 26.1 us  [local(): piece_value = lax.all_gather(w_value, 'sp', axis=0, tiled=True)]
    all_gather x1, waiting for transfers between devices: 1.88 us -> 5.89 us  [local(): piece_conv = lax.all_gather(w_conv_in, 'sp', axis=0, tiled=True)]
    ppermute x0 -> x3, starting transfers between devices: none -> 3.11 us  [local(): lax.ppermute(moving, 'sp', [(i_2, (i_2 + 1) % devices) for i_2 in range(d...]
  transfers between devices with their start and end apart: 9 -> 12, of which waited for: 7 -> 9; matrix products, arithmetic and copies ran while one was open for 7% -> 7% of each run, Pallas kernels for 0% -> 0%
where the time goes in v1:
time: 262 us
  waiting for transfers between devices  185 us (71%)
  blocking collectives  31 us (12%)
  between operations  13.6 us (5%)
  matrix products  13.4 us (5%)
  starting transfers between devices  10.3 us (4%)
  other arithmetic  6.78 us (3%)
    all_gather x1, waiting for transfers between devices, local(): own_whole = lax.all_gather(own_rows, 'sp', axis=1, tiled=True)  66.2 us
    all_gather x1, waiting for transfers between devices, local(): piece_gate = lax.all_gather(w_conv_gate, 'sp', axis=0, tiled=True)  45.6 us
    all_gather x1, waiting for transfers between devices, local(): piece_query = lax.all_gather(w_query, 'sp', axis=0, tiled=True)  39.2 us
    all_gather x1, blocking collectives, local(): piece_value = lax.all_gather(w_value, 'sp', axis=0, tiled=True)  26.1 us
    ppermute x3, waiting for transfers between devices, local(): lax.ppermute(moving, 'sp', [(i_2, (i_2 + 1) % devices) for i_2 in range(d...  10.2 us
    reduce_scatter x1, waiting for transfers between devices, local(): lax.psum_scatter(jnp.dot(features, own_whole, preferred_element_type=jnp....  7.04 us
    ppermute x2, waiting for transfers between devices, padded(): lax.ppermute(lax.slice_in_dim(block, 0, width, axis=dim), axis, backward)  7 us
    all_gather x1, waiting for transfers between devices, local(): piece_conv = lax.all_gather(w_conv_in, 'sp', axis=0, tiled=True)  5.89 us
  transfers between devices with their start and end apart: 12, of which 9 were waited for; matrix products, arithmetic and copies ran while one was open for 7% of the time, Pallas kernels for 0%

profile of v1, /device:TPU:0, one launch (start us, length us, event | category | flops | bytes accessed | tf_op | source)
XLA Modules:
  0.0 261.9 jit_solution(3118901343902812022)
XLA Ops:
  8.8 3.1 %collective-permute-start = (bf16[512,128]{1,0:T(8,128)(2,1)}, bf16[512,128]{1,0:T(8,128)(2,1)S(1)}, u32[]{:S(2)}, u32[]{:S(2)}) collective-permute-start(bf16[512,128]{1,0:T(8,128)(2,1)} %param.17), channel_id=1, source_target_pairs={{0,8},{8,16},{16,24},{24,0},{1,9},{9,17},{17,25},{25,1},{2,10},{10... | collective-permute-start | bytes 393224 | tf_op jit(solution)/shard_map/ppermute | solution.py:85
  11.9 1.3 constant_dynamic-slice_fusion
  13.2 1.0 pad_maximum_fusion
  15.2 2.4 collective-permute-done
  17.6 7.8 %collective-permute-done.1 = bf16[512,128]{1,0:T(8,128)(2,1)S(1)} collective-permute-done((bf16[512,128]{1,0:T(8,128)(2,1)S(1)}, bf16[512,128]{1,0:T(8,128)(2,1)S(1)}, u32[]{:S(2)}, u32[]{:S(2)}) %collective-permute-start.1) | collective-permute-done | bytes 131104 | tf_op jit(solution)/shard_map/ppermute | solution.py:85
  25.4 26.1 %all_gather.15 = bf16[2048,128]{1,0:T(8,128)(2,1)S(1)} all-gather(bf16[512,128]{1,0:T(8,128)(2,1)S(1)} %copy-done.2), channel_id=1, replica_groups=mesh['sp'=4,'fs'=4,'tp'=2] {'sp'}, dimensions={0}, use_global_device_ids=true | all-gather | bytes 655360 | tf_op jit(solution)/shard_map/all_gather | solution.py:89
  52.6 2.4 collective-permute-start.3
  54.9 1.3 collective-permute-start.4
  56.4 1.9 collective-permute-done.3
  58.2 7.0 %collective-permute-done.4 = bf16[128,256]{0,1:T(8,128)(2,1)S(1)} collective-permute-done((bf16[128,256]{0,1:T(8,128)(2,1)S(1)}, bf16[128,256]{0,1:T(8,128)(2,1)S(1)}, u32[]{:S(2)}, u32[]{:S(2)}) %collective-permute-start.4) | collective-permute-done | bytes 65568 | tf_op jit(solution)/shard_map/ppermute | solution.py:22
  65.3 5.9 %all-gather.7.cloned.1.call-done = bf16[2048,512]{1,0:T(8,128)(2,1)} async-done(((bf16[512,512]{1,0:T(8,128)(2,1)}), bf16[2048,512]{1,0:T(8,128)(2,1)}) %all-gather.7.cloned.1.call-update) | async-done | bytes 2097168 | tf_op jit(solution)/shard_map/all_gather | solution.py:90
  71.2 45.6 %all-gather.9.cloned.1.call-done = bf16[2048,512]{1,0:T(8,128)(2,1)} async-done(((bf16[512,512]{1,0:T(8,128)(2,1)}), bf16[2048,512]{1,0:T(8,128)(2,1)}) %all-gather.9.cloned.1.call-update) | async-done | bytes 2097168 | tf_op jit(solution)/shard_map/all_gather | solution.py:91
  116.8 3.5 %fusion = f32[256,1024]{1,0:T(8,128)S(1)} fusion(bf16[2048,512]{1,0:T(8,128)(2,1)} %all-gather.9.cloned.1.call-done, bf16[2048,512]{1,0:T(8,128)(2,1)} %all-gather.7.cloned.1.call-done, bf16[256,2048]{1,0:T(8,128)(2,1)S(1)} %copy-done, f32[2048]{0:T(1024)S(1)} %copy-done.7, f32[256]{0:T(256)S(1)} %add_rsqrt_fusion.1), kind=kOutput, calls=%fused_computation | convolution fusion | flops 1084227584 | bytes 6300672 | tf_op jit(solution)/shard_map/dot_general | solution.py:98
  120.5 2.1 collective-permute-start.5
  122.6 1.3 collective-permute-start.6
  123.9 39.2 %all-gather.5.cloned.1.call-done = bf16[2048,512]{1,0:T(8,128)(2,1)} async-done(((bf16[512,512]{1,0:T(8,128)(2,1)}), bf16[2048,512]{1,0:T(8,128)(2,1)}) %all-gather.5.cloned.1.call-update) | async-done | bytes 2097168 | tf_op jit(solution)/shard_map/all_gather | solution.py:81
  163.0 2.6 %fusion.74 = f32[256,512]{0,1:T(8,128)S(1)} fusion(bf16[2048,512]{1,0:T(8,128)(2,1)} %all-gather.5.cloned.1.call-done, bf16[256,2048]{1,0:T(8,128)(2,1)S(1)} %copy-done, f32[2048]{0:T(1024)S(1)} %copy-done.7, f32[256]{0:T(256)S(1)} %add_rsqrt_fusion.1), kind=kOutput, calls=%fused_computation.175 | convolution fusion | flops 538968064 | bytes 3679232 | tf_op jit(solution)/shard_map/dot_general | solution.py:92
  167.7 1.2 fusion.10
  169.1 3.1 %fusion.77 = (f32[256]{0:T(256)S(1)}, f32[256,512]{1,0:T(8,128)S(1)}) fusion(bf16[15,512]{1,0:T(8,128)(2,1)S(1)} %collective-permute-done.6, bf16[256,512]{1,0:T(8,128)(2,1)S(1)} %fusion.22, f32[512]{0:T(512)S(1)} %bitcast.106, f32[512]{0:T(512)S(1)} %bitcast.107, f32[512]{0:T(512)S(1)} %bitcast.78, f32[512]{0:T(512)S(1)} %bitcast.79, f32[512]{0:T(512)S(1)} %bitcast.80, ...), kind=kLoop, calls=%fused_computation.176 | loop fusion | flops 24116992 | bytes 883712 | tf_op jit(solution)/shard_map/reduce_sum | solution.py:147
  172.2 2.5 psum.14
  174.9 2.5 psum.15
  177.6 66.2 %all-gather.11.cloned.1.call-done = bf16[1024,2048]{1,0:T(8,128)(2,1)} async-done(((bf16[1024,512]{1,0:T(8,128)(2,1)}), bf16[1024,2048]{1,0:T(8,128)(2,1)}) %all-gather.11.cloned.1.call-update) | async-done | bytes 4194320 | tf_op jit(solution)/shard_map/all_gather | solution.py:162
  243.9 4.5 %convolution_convert_fusion = bf16[256,2048]{1,0:T(8,128)(2,1)} fusion(bf16[1024,2048]{1,0:T(8,128)(2,1)} %all-gather.11.cloned.1.call-done, bf16[256,512]{1,0:T(8,128)(2,1)S(1)} %multiply_convert_fusion, bf16[256,512]{1,0:T(8,128)(2,1)S(1)} %copy.27), kind=kOutput, calls=%fused_computation.11 | convolution fusion | flops 1075314688 | bytes 5767168 | tf_op jit(solution)/shard_map/dot_general | solution.py:164
  248.4 7.0 %reduce-scatter.2.cloned.1.call-done = bf16[128,2048]{1,0:T(8,128)(2,1)} async-done(((bf16[256,2048]{1,0:T(8,128)(2,1)}), bf16[128,2048]{1,0:T(8,128)(2,1)}) %reduce-scatter.2.cloned.1.call-update) | async-done | bytes 524304 | tf_op jit(solution)/shard_map/reduce_scatter | solution.py:163
  (74 shorter events, 7.0 us)
Async XLA Ops:
  6.5 7.9 %copy-start.3 = (f32[31,512]{1,0:T(8,128)S(1)}, f32[31,512]{1,0:T(8,128)}, u32[]{:S(2)}) copy-start(f32[31,512]{1,0:T(8,128)} %param.22) | copy-start | bytes 190468
  6.5 8.4 %copy-start = (bf16[256,2048]{1,0:T(8,128)(2,1)S(1)}, bf16[256,2048]{1,0:T(8,128)(2,1)}, u32[]{:S(2)}) copy-start(bf16[256,2048]{1,0:T(8,128)(2,1)} %param.14) | copy-start | bytes 3145732
  6.5 18.9 %copy-start.2 = (bf16[512,128]{1,0:T(8,128)(2,1)S(1)}, bf16[512,128]{1,0:T(8,128)(2,1)}, u32[]{:S(2)}) copy-start(bf16[512,128]{1,0:T(8,128)(2,1)} %param.18) | copy-start | bytes 393220
  6.5 64.6 %all-gather.7.cloned.1.call-start = ((), (), s32[]{:S(2)}) async-start(), calls=%async_computation.2 | async-start | bytes 2621440 | tf_op jit(solution)/shard_map/all_gather | solution.py:90
  7.3 109.5 %all-gather.9.cloned.1.call-start = ((), (), s32[]{:S(2)}) async-start(), calls=%async_computation.3 | async-start | bytes 2621440 | tf_op jit(solution)/shard_map/all_gather | solution.py:91
  8.0 43.6 %copy-start.1 = (bf16[512,128]{1,0:T(8,128)(2,1)S(1)}, bf16[512,128]{1,0:T(8,128)(2,1)}, u32[]{:S(2)}) copy-start(bf16[512,128]{1,0:T(8,128)(2,1)} %param.17) | copy-start | bytes 393220
  8.0 155.0 %all-gather.5.cloned.1.call-start = ((), (), s32[]{:S(2)}) async-start(), calls=%async_computation.1 | async-start | bytes 2621440 | tf_op jit(solution)/shard_map/all_gather | solution.py:81
  8.8 235.1 %all-gather.11.cloned.1.call-start = ((), (), s32[]{:S(2)}) async-start(), calls=%async_computation.4 | async-start | bytes 5242880 | tf_op jit(solution)/shard_map/all_gather | solution.py:162
  8.8 8.8 %collective-permute-start = (bf16[512,128]{1,0:T(8,128)(2,1)}, bf16[512,128]{1,0:T(8,128)(2,1)S(1)}, u32[]{:S(2)}, u32[]{:S(2)}) collective-permute-start(bf16[512,128]{1,0:T(8,128)(2,1)} %param.17), channel_id=1, source_target_pairs={{0,8},{8,16},{16,24},{24,0},{1,9},{9,17},{17,25},{25,1},{2,10},{10... | collective-permute-start | bytes 393224 | tf_op jit(solution)/shard_map/ppermute | solution.py:85
  13.2 38.6 %copy-start.7 = (f32[2048]{0:T(1024)S(1)}, f32[2048]{0:T(1024)}, u32[]{:S(2)}) copy-start(f32[2048]{0:T(1024)} %param.15) | copy-start | bytes 24580
  14.3 241.1 %reduce-scatter.2.cloned.1.call-start = ((), (), s32[]{:S(2)}) async-start(), calls=%async_computation.5 | async-start | bytes 1572864 | tf_op jit(solution)/shard_map/reduce_scatter | solution.py:163
  17.6 7.8 %collective-permute-start.1 = (bf16[512,128]{1,0:T(8,128)(2,1)S(1)}, bf16[512,128]{1,0:T(8,128)(2,1)S(1)}, u32[]{:S(2)}, u32[]{:S(2)}) collective-permute-start(bf16[512,128]{1,0:T(8,128)(2,1)S(1)} %collective-permute-done), channel_id=1, source_target_pairs={{0,8},{8,16},{16,24},{24,0},{1,9},{9,17},{17,25},{25,1},{2,10},{10... | collective-permute-start | bytes 393224 | tf_op jit(solution)/shard_map/ppermute | solution.py:85
  25.4 26.1 %collective-permute-start.2 = (bf16[512,128]{1,0:T(8,128)(2,1)S(1)}, bf16[512,128]{1,0:T(8,128)(2,1)S(1)}, u32[]{:S(2)}, u32[]{:S(2)}) collective-permute-start(bf16[512,128]{1,0:T(8,128)(2,1)S(1)} %collective-permute-done.1), channel_id=1, source_target_pairs={{0,8},{8,16},{16,24},{24,0},{1,9},{9,17},{17,25},{25,1},{2,10},{10... | collective-permute-start | bytes 393224 | tf_op jit(solution)/shard_map/ppermute | solution.py:85
  51.5 4.8 %copy-start.8 = (f32[8]{0:T(128)S(1)}, f32[8]{0:T(128)}, u32[]{:S(2)}) copy-start(f32[8]{0:T(128)} %param.21) | copy-start | bytes 100
  52.6 5.7 %collective-permute-start.3 = (bf16[128,256]{0,1:T(8,128)(2,1)S(1)}, bf16[128,256]{0,1:T(8,128)(2,1)S(1)}, u32[]{:S(2)}, u32[]{:S(2)}) collective-permute-start(bf16[128,256]{0,1:T(8,128)(2,1)S(1)} %get-tuple-element.21), channel_id=1, source_target_pairs={{0,8},{8,16},{16,24},{1,9},{9,17},{17,25},{2,10},{10,18},{18,26},{... | collective-permute-start | bytes 196616 | tf_op jit(solution)/shard_map/ppermute | solution.py:19
  54.9 10.3 %collective-permute-start.4 = (bf16[128,256]{0,1:T(8,128)(2,1)S(1)}, bf16[128,256]{0,1:T(8,128)(2,1)S(1)}, u32[]{:S(2)}, u32[]{:S(2)}) collective-permute-start(bf16[128,256]{0,1:T(8,128)(2,1)S(1)} %get-tuple-element.22), channel_id=1, source_target_pairs={{8,0},{16,8},{24,16},{9,1},{17,9},{25,17},{10,2},{18,10},{26,18},{... | collective-permute-start | bytes 196616 | tf_op jit(solution)/shard_map/ppermute | solution.py:22
  120.5 48.6 %collective-permute-start.5 = (bf16[15,512]{1,0:T(8,128)(2,1)S(1)}, bf16[15,512]{1,0:T(8,128)(2,1)S(1)}, u32[]{:S(2)}, u32[]{:S(2)}) collective-permute-start(bf16[15,512]{1,0:T(8,128)(2,1)S(1)} %get-tuple-element.15), channel_id=1, source_target_pairs={{0,8},{8,16},{16,24},{1,9},{9,17},{17,25},{2,10},{10,18},{18,26},{... | collective-permute-start | bytes 46088 | tf_op jit(solution)/shard_map/ppermute | solution.py:19
  122.6 46.5 %collective-permute-start.6 = (bf16[15,512]{1,0:T(8,128)(2,1)S(1)}, bf16[15,512]{1,0:T(8,128)(2,1)S(1)}, u32[]{:S(2)}, u32[]{:S(2)}) collective-permute-start(bf16[15,512]{1,0:T(8,128)(2,1)S(1)} %get-tuple-element.16), channel_id=1, source_target_pairs={{8,0},{16,8},{24,16},{9,1},{17,9},{25,17},{10,2},{18,10},{26,18},{... | collective-permute-start | bytes 46088 | tf_op jit(solution)/shard_map/ppermute | solution.py:22
  167.6 1.4 copy-start.4
  167.6 9.7 %copy-start.5 = (f32[512]{0:T(512)S(1)}, f32[512]{0:T(512)}, u32[]{:S(2)}) copy-start(f32[512]{0:T(512)} %param.25) | copy-start | bytes 6148
  167.6 9.7 %copy-start.6 = (f32[512]{0:T(512)S(1)}, f32[512]{0:T(512)}, u32[]{:S(2)}) copy-start(f32[512]{0:T(512)} %param.24) | copy-start | bytes 6148
Sparse Core Ops, SparseCore 0:
  8.9 62.2 all-gather.6
  72.7 43.9 all-gather.8
  118.4 44.6 all-gather.4
  164.5 79.3 all-gather.10
  248.5 6.8 reduce-scatter.1
